TPU v7x, 32 devices: a whole 2x2x4 slice. The times are simulated.
32 devices in a mesh: rep: 2 (over x), fs: 8 (over z, y), tp: 2 (over core).
Axes of the slice: x: 2, y: 2, z: 4, core: 2. Of those that a mesh axis runs over, the one named last changes fastest.
Arguments:
- tokens: bfloat16 [5120, 2048], P(('rep', 'fs')), may hold values from -6 to 6
- mixer_out: bfloat16 [5120, 2048], P(('rep', 'fs')), may hold values from -6 to 6
- gate_first: bfloat16 [2048, 2816], P('fs', 'tp'), may hold values from -0.125 to 0.125
- up_first: bfloat16 [2048, 2816], P('fs', 'tp'), may hold values from -0.125 to 0.125
- down_first: bfloat16 [2816, 2048], P('tp', 'fs'), may hold values from -0.3125 to 0.3125
- gate_second: bfloat16 [2048, 2816], P('fs', 'tp'), may hold values from -0.125 to 0.125
- up_second: bfloat16 [2048, 2816], P('fs', 'tp'), may hold values from -0.125 to 0.125
- down_second: bfloat16 [2816, 2048], P('tp', 'fs'), may hold values from -0.3125 to 0.3125
- gain_first: float32 [2048], replicated, may hold values from 0.1 to 1.9
- bias_first: float32 [2048], replicated, may hold values from -1.5 to 1.5
- gain_middle: float32 [2048], replicated, may hold values from 0.1 to 1.9
- bias_middle: float32 [2048], replicated, may hold values from -1.5 to 1.5
- gain_last: float32 [2048], replicated, may hold values from 0.1 to 1.9
- bias_last: float32 [2048], replicated, may hold values from -1.5 to 1.5
Outputs:
- layer_out: bfloat16 [5120, 2048], P(('rep', 'fs'))
All inputs are finite; a program needn't handle non-finite values.
Results may differ from a plain program's by a relative error of at most 0.014.
Values may be sent and summed in bfloat16 or wider, within the bound.
No kernel may reach another device: no remote copies, remote signals or barrier semaphores. Data moves between devices by JAX's collectives and lax.ppermute only.
A program may use at most 64 MiB of HBM per device.

v0:
```python
import math

import jax
import jax.numpy as jnp
from jax import lax
from jax.sharding import PartitionSpec as P

residual_scale = math.sqrt(2.0)
norm_eps = 1e-05


def normalize(summed, scaling, offset):
    center = summed - jnp.mean(summed, axis=-1, keepdims=True)
    spread = jnp.mean(center * center, axis=-1, keepdims=True)
    return center * lax.rsqrt(spread + norm_eps) * scaling + offset


def add_columns(inputs, portion):
    return jnp.dot(inputs, portion, preferred_element_type=jnp.float32)


def project_in(inputs, gate_weight, up_weight):
    return (
        add_columns(inputs, lax.all_gather(gate_weight, "fs", axis=0, tiled=True)),
        add_columns(inputs, lax.all_gather(up_weight, "fs", axis=0, tiled=True)),
    )


def project_out(hidden, down_weight):
    return jnp.dot(
        hidden,
        lax.all_gather(down_weight, "fs", axis=1, tiled=True),
        preferred_element_type=jnp.float32,
    )


def half_step(inputs, gate_weight, up_weight, down_weight):
    gate, value = project_in(inputs, gate_weight, up_weight)
    hidden = (jax.nn.silu(gate) * value).astype(jnp.bfloat16)
    partials = project_out(hidden, down_weight)
    summed = lax.psum(partials.astype(jnp.bfloat16), "tp")
    return summed


def per_device(
    tokens,
    mixer_out,
    gate_first,
    up_first,
    down_first,
    gate_second,
    up_second,
    down_second,
    gain_first,
    bias_first,
    gain_middle,
    bias_middle,
    gain_last,
    bias_last,
):
    first_branch = half_step(tokens, gate_first, up_first, down_first)
    first_norm = normalize(
        residual_scale * tokens.astype(jnp.float32) + 0.5 * first_branch.astype(jnp.float32),
        gain_first,
        bias_first,
    ).astype(jnp.bfloat16)
    middle_norm = normalize(
        residual_scale * first_norm.astype(jnp.float32) + mixer_out.astype(jnp.float32),
        gain_middle,
        bias_middle,
    ).astype(jnp.bfloat16)
    second_branch = half_step(middle_norm, gate_second, up_second, down_second)
    finished = normalize(
        residual_scale * middle_norm.astype(jnp.float32) + 0.5 * second_branch.astype(jnp.float32),
        gain_last,
        bias_last,
    ).astype(jnp.bfloat16)
    return finished


def solution(mesh):
    return jax.shard_map(
        per_device,
        mesh=mesh,
        in_specs=(
            P(("rep", "fs"), None),
            P(("rep", "fs"), None),
            P("fs", "tp"),
            P("fs", "tp"),
            P("tp", "fs"),
            P("fs", "tp"),
            P("fs", "tp"),
            P("tp", "fs"),
            P(),
            P(),
            P(),
            P(),
            P(),
            P(),
        ),
        out_specs=P(("rep", "fs"), None),
        check_vma=False,
    )
```

profile of v0, /device:TPU:0, one launch (start us, length us, event | category | flops | bytes accessed | tf_op | source)
XLA Modules:
  0.0 639.6 jit_solution(13720102844049315975)
XLA Ops:
  6.5 0.7 all-gather.7.cloned.1.call-update
  7.3 0.0 all-gather.11.cloned.1.call-start
  7.3 0.7 all-gather.11.cloned.1.call-update
  8.0 0.0 all-gather.9.cloned.1.call-start
  8.1 0.7 all-gather.9.cloned.1.call-update
  8.8 0.0 all-reduce.3.cloned.1.call-start
  8.8 95.8 %all-gather.7.cloned.1.call-done = bf16[2048,1408]{1,0:T(8,128)(2,1)} async-done(((bf16[256,1408]{1,0:T(8,128)(2,1)}), bf16[2048,1408]{1,0:T(8,128)(2,1)}) %all-gather.7.cloned.1.call-update) | async-done | bytes 5767184 | tf_op jit(solution)/shard_map/all_gather | solution.py:24
  104.6 5.2 fusion.7
  109.8 88.2 %all-gather.11.cloned.1.call-done = bf16[1408,2048]{1,0:T(8,128)(2,1)} async-done(((bf16[1408,256]{1,0:T(8,128)(2,1)}), bf16[1408,2048]{1,0:T(8,128)(2,1)}) %all-gather.11.cloned.1.call-update) | async-done | bytes 5767184 | tf_op jit(solution)/shard_map/all_gather | solution.py:32
  198.0 92.7 %all-gather.9.cloned.1.call-done = bf16[2048,1408]{1,0:T(8,128)(2,1)} async-done(((bf16[256,1408]{1,0:T(8,128)(2,1)}), bf16[2048,1408]{1,0:T(8,128)(2,1)}) %all-gather.9.cloned.1.call-update) | async-done | bytes 5767184 | tf_op jit(solution)/shard_map/all_gather | solution.py:25
  290.7 9.7 %convolution_convert_fusion.1 = bf16[320,2048]{1,0:T(8,128)(2,1)} fusion(bf16[1408,2048]{1,0:T(8,128)(2,1)} %all-gather.11.cloned.1.call-done, bf16[320,2048]{1,0:T(8,128)(2,1)S(1)} %copy-done.2, bf16[2048,1408]{1,0:T(8,128)(2,1)} %all-gather.9.cloned.1.call-done, f32[320,1408]{1,0:T(8,128)S(1)} %fusion.7), kind=kOutput, calls=%fused_computation.3 | convolution fusion | flops 3694346240 | bytes 15958016 | tf_op jit(solution)/shard_map/dot_general | solution.py:30
  300.4 0.0 all-gather.13.cloned.1.call-start
  300.4 0.5 all-gather.13.cloned.1.call-update
  301.0 0.0 all-gather.15.cloned.1.call-start
  301.0 0.5 all-gather.15.cloned.1.call-update
  301.6 0.7 all-gather.17.cloned.1.call-update
  302.3 0.2 all-reduce.5.cloned.1.call-start
  302.5 16.1 %all-reduce.3.cloned.1.call-done = bf16[320,2048]{1,0:T(8,128)(2,1)} async-done(((bf16[320,2048]{1,0:T(8,128)(2,1)}), bf16[320,2048]{1,0:T(8,128)(2,1)}) %all-reduce.3.cloned.1.call-update) | async-done | bytes 1310736 | tf_op jit(solution)/shard_map/psum | solution.py:41
  318.6 2.0 fusion.3
  320.6 0.8 multiply_reduce_fusion.2
  321.5 1.3 fusion.2
  322.8 0.7 multiply_reduce_fusion.1
  323.5 0.8 add_convert_fusion.1
  324.3 89.9 %all-gather.13.cloned.1.call-done = bf16[2048,1408]{1,0:T(8,128)(2,1)} async-done(((bf16[256,1408]{1,0:T(8,128)(2,1)}), bf16[2048,1408]{1,0:T(8,128)(2,1)}) %all-gather.13.cloned.1.call-update) | async-done | bytes 5767184 | tf_op jit(solution)/shard_map/all_gather | solution.py:24
  414.2 4.8 fusion.8
  419.0 87.7 %all-gather.15.cloned.1.call-done = bf16[2048,1408]{1,0:T(8,128)(2,1)} async-done(((bf16[256,1408]{1,0:T(8,128)(2,1)}), bf16[2048,1408]{1,0:T(8,128)(2,1)}) %all-gather.15.cloned.1.call-update) | async-done | bytes 5767184 | tf_op jit(solution)/shard_map/all_gather | solution.py:25
  506.7 93.4 %all-gather.17.cloned.1.call-done = bf16[1408,2048]{1,0:T(8,128)(2,1)} async-done(((bf16[1408,256]{1,0:T(8,128)(2,1)}), bf16[1408,2048]{1,0:T(8,128)(2,1)}) %all-gather.17.cloned.1.call-update) | async-done | bytes 5767184 | tf_op jit(solution)/shard_map/all_gather | solution.py:32
  600.1 9.7 %convolution_convert_fusion = bf16[320,2048]{1,0:T(8,128)(2,1)} fusion(bf16[1408,2048]{1,0:T(8,128)(2,1)} %all-gather.17.cloned.1.call-done, bf16[320,2048]{1,0:T(8,128)(2,1)S(1)} %add_convert_fusion.1, bf16[2048,1408]{1,0:T(8,128)(2,1)} %all-gather.15.cloned.1.call-done, f32[320,1408]{1,0:T(8,128)S(1)} %fusion.8), kind=kOutput, calls=%fused_computation.2 | convolution fusion | flops 3694346240 | bytes 15958016 | tf_op jit(solution)/shard_map/dot_general | solution.py:30
  609.8 18.2 %all-reduce.5.cloned.1.call-done = bf16[320,2048]{1,0:T(8,128)(2,1)} async-done(((bf16[320,2048]{1,0:T(8,128)(2,1)}), bf16[320,2048]{1,0:T(8,128)(2,1)}) %all-reduce.5.cloned.1.call-update) | async-done | bytes 1310736 | tf_op jit(solution)/shard_map/psum | solution.py:41
  628.0 2.0 fusion.4
  630.0 0.8 multiply_reduce_fusion
  630.9 1.9 add_convert_fusion
  (30 shorter events, 0.2 us)
Async XLA Ops:
  6.5 98.0 %all-gather.7.cloned.1.call-start = ((), (), s32[]{:S(2)}) async-start(), calls=%async_computation | async-start | bytes 6488064 | tf_op jit(solution)/shard_map/all_gather | solution.py:24
  7.3 190.7 %all-gather.11.cloned.1.call-start = ((), (), s32[]{:S(2)}) async-start(), calls=%async_computation.2 | async-start | bytes 6488064 | tf_op jit(solution)/shard_map/all_gather | solution.py:32
  8.0 282.7 %all-gather.9.cloned.1.call-start = ((), (), s32[]{:S(2)}) async-start(), calls=%async_computation.1 | async-start | bytes 6488064 | tf_op jit(solution)/shard_map/all_gather | solution.py:25
  8.7 281.9 %copy-start.2 = (bf16[320,2048]{1,0:T(8,128)(2,1)S(1)}, bf16[320,2048]{1,0:T(8,128)(2,1)}, u32[]{:S(2)}) copy-start(bf16[320,2048]{1,0:T(8,128)(2,1)} %param.14) | copy-start | bytes 3932164
  8.8 309.8 %all-reduce.3.cloned.1.call-start = ((), (), s32[]{:S(2)}) async-start(), calls=%async_computation.3 | async-start | bytes 2621440 | tf_op jit(solution)/shard_map/psum | solution.py:41
  300.4 113.8 %all-gather.13.cloned.1.call-start = ((), (), s32[]{:S(2)}) async-start(), calls=%async_computation.4 | async-start | bytes 6488064 | tf_op jit(solution)/shard_map/all_gather | solution.py:24
  301.0 205.8 %all-gather.15.cloned.1.call-start = ((), (), s32[]{:S(2)}) async-start(), calls=%async_computation.5 | async-start | bytes 6488064 | tf_op jit(solution)/shard_map/all_gather | solution.py:25
  301.5 298.6 %all-gather.17.cloned.1.call-start = ((), (), s32[]{:S(2)}) async-start(), calls=%async_computation.6 | async-start | bytes 6488064 | tf_op jit(solution)/shard_map/all_gather | solution.py:32
  301.6 19.9 %copy-start.4 = (f32[2048]{0:T(1024)S(1)}, f32[2048]{0:T(1024)}, u32[]{:S(2)}) copy-start(f32[2048]{0:T(1024)} %param.23) | copy-start | bytes 24580
  301.6 19.9 %copy-start.5 = (f32[2048]{0:T(1024)S(1)}, f32[2048]{0:T(1024)}, u32[]{:S(2)}) copy-start(f32[2048]{0:T(1024)} %param.22) | copy-start | bytes 24580
  302.3 19.2 %copy-start.1 = (bf16[320,2048]{1,0:T(8,128)(2,1)S(1)}, bf16[320,2048]{1,0:T(8,128)(2,1)}, u32[]{:S(2)}) copy-start(bf16[320,2048]{1,0:T(8,128)(2,1)} %param.15) | copy-start | bytes 3932164
  302.3 325.7 %all-reduce.5.cloned.1.call-start = ((), (), s32[]{:S(2)}) async-start(), calls=%async_computation.7 | async-start | bytes 2621440 | tf_op jit(solution)/shard_map/psum | solution.py:41
  318.6 2.0 copy-start.3
  322.8 0.7 copy-start.6
  322.8 0.7 copy-start.7
  609.8 21.0 %copy-start.8 = (f32[2048]{0:T(1024)S(1)}, f32[2048]{0:T(1024)}, u32[]{:S(2)}) copy-start(f32[2048]{0:T(1024)} %param.27) | copy-start | bytes 24580
  609.8 21.0 %copy-start.9 = (f32[2048]{0:T(1024)S(1)}, f32[2048]{0:T(1024)}, u32[]{:S(2)}) copy-start(f32[2048]{0:T(1024)} %param.26) | copy-start | bytes 24580
  628.0 2.0 copy-start
Sparse Core Ops, SparseCore 0:
  9.5 95.0 all-gather.6
  106.6 91.3 all-gather.10
  200.2 90.4 all-gather.8
  300.5 18.0 all-reduce.2
  320.6 93.4 all-gather.12
  416.2 90.4 all-gather.14
  508.8 91.2 all-gather.16
  609.9 18.0 all-reduce.4
where the time goes:
time: 640 us
  waiting for transfers between devices  586 us (92%)
  matrix products  29.4 us (5%)
  between operations  13.6 us (2%)
  other arithmetic  10.4 us (2%)
    all_gather x2, waiting for transfers between devices, project_in(): lax.all_gather(gate_weight, 'fs', axis=0, tiled=True)  186 us
    all_gather x2, waiting for transfers between devices, project_out(): lax.all_gather(down_weight, 'fs', axis=1, tiled=True)  182 us
    all_gather x2, waiting for transfers between devices, project_in(): lax.all_gather(up_weight, 'fs', axis=0, tiled=True)  180 us
    psum x2, waiting for transfers between devices, half_step(): summed = lax.psum(partials.astype(jnp.bfloat16), 'tp')  34.3 us
    dot_general x2, matrix products, project_out(): jnp.dot(hidden, lax.all_gather(down_weight, 'fs', axis=1, tiled=True), pr...  19.3 us
  transfers between devices with their start and end apart: 8, of which 8 were waited for; matrix products, arithmetic and copies ran while one was open for 2% of the time, Pallas kernels for 0%

commit v1 on v0

v1 whole, which is shorter than its diff:
```python
import math

import jax
import jax.numpy as jnp
from jax import lax
from jax.sharding import PartitionSpec as P

residual_scale = math.sqrt(2.0)
norm_eps = 1e-05
bf16, f32 = jnp.bfloat16, jnp.float32


def make_body(R, F, C):
    m = F // 2
    NG = 2 * R

    def body(tokens, mixer_out, gate_first, up_first, down_first, gate_second,
             up_second, down_second, gain_first, bias_first, gain_middle,
             bias_middle, gain_last, bias_last):
        a = lax.axis_index("rep")
        i = lax.axis_index("fs")
        c = lax.axis_index("tp")
        z, b = i // 2, i % 2
        g = a * 2 + b

        def pair_swap(x):
            return lax.ppermute(x, "fs", [(j, j ^ 1) for j in range(F)])

        def tp_shift(x, k):
            return lax.ppermute(x, "tp", [(j, (j + k) % C) for j in range(C)])

        def plane_xor(x, k, only=None):
            pairs = [(j, j ^ (2 * k)) for j in range(F) if only is None or (j // 2) in only]
            return lax.ppermute(x, "fs", pairs)

        def group_xor(x, d):
            dr, dy = d // 2, d % 2
            pairs = [(r * F + j, (r ^ dr) * F + (j ^ dy)) for r in range(R) for j in range(F)]
            return lax.ppermute(x, ("rep", "fs"), pairs)

        rows = tokens.shape[0]
        h = rows // C
        D = tokens.shape[1]
        kb = D // m
        ffl = gate_first.shape[1]
        piece = ffl // NG

        hid = lax.broadcasted_iota(jnp.int32, (piece, ffl), 1)
        row = lax.broadcasted_iota(jnp.int32, (piece, ffl), 0)

        def pick_in(w, which):
            sel = (hid == row + which * piece).astype(bf16)
            return lax.dot_general(sel, w, (((1,), (1,)), ((), ())),
                                   preferred_element_type=f32).astype(bf16)

        def pick_down(w, which):
            return lax.dynamic_slice_in_dim(w, which * piece, piece, axis=0)

        def ordered(own, other):
            lo = jnp.where(b == 0, own, other)
            hi = jnp.where(b == 0, other, own)
            return jnp.concatenate([lo, hi], axis=1)

        mine, theirs = g, a * 2 + (1 - b)

        def in_block(gw, uw):
            own = jnp.concatenate([pick_in(gw, mine), pick_in(uw, mine)], axis=0)
            away = jnp.concatenate([pick_in(gw, theirs), pick_in(uw, theirs)], axis=0)
            return ordered(own, pair_swap(away))

        def down_block(dw):
            return ordered(pick_down(dw, mine), pair_swap(pick_down(dw, theirs)))

        def planes(x):
            if m != 4:
                return [x] + [plane_xor(x, k) for k in range(1, m)]
            one = plane_xor(x, 1)
            two = plane_xor(x, 2)
            mid = plane_xor(x, 3, only=(1, 2))
            far = lax.ppermute(two, "fs", [(2, 0), (3, 1), (4, 6), (5, 7)])
            three = jnp.where((z == 1) | (z == 2), mid, far)
            return [x, one, two, three]

        def half(x):
            return lax.dynamic_slice_in_dim(x, c * h, h, axis=0)

        def by_block(x):
            return x.reshape(x.shape[0], m, kb).transpose(1, 0, 2)

        def gather_tokens(x):
            same = jnp.concatenate([x] + [group_xor(x, d) for d in range(1, NG)], axis=1)
            return jnp.concatenate([same] + [tp_shift(same, k) for k in range(1, C)], axis=1)

        def block_of(x, k):
            return lax.dynamic_index_in_dim(x, z ^ k, 0, keepdims=False)

        def contract(x, w):
            return lax.dot_general(x, w, (((1,), (1,)), ((), ())), preferred_element_type=f32)

        def hidden_of(u, ws):
            gate = up = None
            for k in range(m):
                x = block_of(u, k)
                p, q = contract(x, ws[k][:piece]), contract(x, ws[k][piece:])
                gate = p if gate is None else gate + p
                up = q if up is None else up + q
            return (jax.nn.silu(gate) * up).astype(bf16)

        def scatter_sum(part):
            part = part.astype(bf16)
            n = NG * h
            acc = part[:n].astype(f32)
            for k in range(1, C):
                acc = acc + tp_shift(part[(C - k) * n:(C - k + 1) * n], k).astype(f32)
            acc16 = acc.astype(bf16)
            out = acc[:h]
            for d in range(1, NG):
                out = out + group_xor(acc16[d * h:(d + 1) * h], d).astype(f32)
            return out

        def feed_forward(u, wi, wd):
            hid16 = hidden_of(u, wi)
            outs = []
            for k in range(m):
                part = jnp.dot(hid16, wd[k], preferred_element_type=f32)
                outs.append(scatter_sum(part).astype(bf16))
            return outs

        def natural(outs):
            st = jnp.stack(outs)
            return jnp.stack([lax.dynamic_index_in_dim(st, z ^ j, 0, keepdims=False)
                              for j in range(m)])

        def vec(v):
            return v.reshape(m, 1, kb)

        def norm(x, gain, bias):
            center = x - jnp.mean(x, axis=(0, 2), keepdims=True)
            spread = jnp.mean(center * center, axis=(0, 2), keepdims=True)
            return center * lax.rsqrt(spread + norm_eps) * vec(gain) + vec(bias)

        tok = by_block(half(tokens))
        mix = by_block(half(mixer_out))
        w1 = planes(in_block(gate_first, up_first))
        u1 = gather_tokens(tok)
        d1 = planes(down_block(down_first))
        w2 = planes(in_block(gate_second, up_second))
        d2 = planes(down_block(down_second))

        branch = natural(feed_forward(u1, w1, d1)).astype(f32)
        first_norm = norm(residual_scale * tok.astype(f32) + 0.5 * branch,
                          gain_first, bias_first).astype(bf16)
        middle = norm(residual_scale * first_norm.astype(f32) + mix.astype(f32),
                      gain_middle, bias_middle).astype(bf16)
        u2 = gather_tokens(middle)
        branch = natural(feed_forward(u2, w2, d2)).astype(f32)
        done = norm(residual_scale * middle.astype(f32) + 0.5 * branch,
                    gain_last, bias_last).astype(bf16)
        done = done.transpose(1, 0, 2).reshape(h, D)
        st = jnp.stack([done] + [tp_shift(done, k) for k in range(1, C)])
        return jnp.concatenate([lax.dynamic_index_in_dim(st, (c - j) % C, 0, keepdims=False)
                                for j in range(C)], axis=0)

    return body


def solution(mesh):
    R, F, C = mesh.shape["rep"], mesh.shape["fs"], mesh.shape["tp"]
    tok = P(("rep", "fs"), None)
    win, wout = P("fs", "tp"), P("tp", "fs")
    return jax.shard_map(
        make_body(R, F, C),
        mesh=mesh,
        in_specs=(tok, tok, win, win, wout, win, win, wout) + (P(),) * 6,
        out_specs=tok,
        check_vma=False,
    )
```

time: 640 us -> 374 us (0.58)
  waiting for transfers between devices: 586 us -> 225 us
  starting transfers between devices: 0.45 us -> 78.8 us
  local copies, waits for them, and re-layouts: 0.05 us -> 16.2 us
  between operations: 13.6 us -> 1.09 us
  other arithmetic: 10.4 us -> 21.8 us
    all_gather x6 -> x0, waiting for transfers between devices: 548 us -> none  [the longest x2 186 us: project_in(): lax.all_gather(gate_weight, 'fs', axis=0, tiled=True)]
    ppermute x0 -> x61, waiting for transfers between devices: none -> 225 us  [the longest x12 141 us: plane_xor(): return lax.ppermute(x, 'fs', pairs)]
    ppermute x0 -> x61, starting transfers between devices: none -> 78.8 us  [the longest x30 42.1 us: group_xor(): return lax.ppermute(x, ('rep', 'fs'), pairs)]
    psum x2 -> x0, waiting for transfers between devices: 34.3 us -> none  [half_step(): summed = lax.psum(partials.astype(jnp.bfloat16), 'tp')]
    concatenate x0 -> x9, other arithmetic: none -> 8.87 us  [the longest x2 4.31 us: gather_tokens(): jnp.concatenate([x] + [group_xor(x, d) for d in range(1, NG)], axis=1)]
    unnamed x20 -> x47, local copies, waits for them, and re-layouts: 0.05 us -> 6.57 us
    dot_general x4 -> x32, matrix products: 29.4 us -> 30.2 us  [the longest x16 17 us: contract(): lax.dot_general(x, w, (((1,), (1,)), ((), ())), preferred_element_type=f32)]
  transfers between devices with their start and end apart: 8 -> 61, of which waited for: 8 -> 31; matrix products, arithmetic and copies ran while one was open for 2% -> 16% of each run, Pallas kernels for 0% -> 0%
where the time goes in v1:
time: 374 us; the launch traced here: 373 us
  waiting for transfers between devices  225 us (60%)
  starting transfers between devices  78.8 us (21%)
  matrix products  30.2 us (8%)
  other arithmetic  21.8 us (6%)
  local copies, waits for them, and re-layouts  16.2 us (4%)
    ppermute x12, waiting for transfers between devices, plane_xor(): return lax.ppermute(x, 'fs', pairs)  141 us
    ppermute x30, waiting for transfers between devices, group_xor(): return lax.ppermute(x, ('rep', 'fs'), pairs)  77.4 us
    ppermute x30, starting transfers between devices, group_xor(): return lax.ppermute(x, ('rep', 'fs'), pairs)  42.1 us
    ppermute x12, starting transfers between devices, plane_xor(): return lax.ppermute(x, 'fs', pairs)  22 us
    dot_general x16, matrix products, contract(): lax.dot_general(x, w, (((1,), (1,)), ((), ())), preferred_element_type=f32)  17 us
    dot_general x8, matrix products, feed_forward(): part = jnp.dot(hid16, wd[k], preferred_element_type=f32)  7.98 us
  transfers between devices with their start and end apart: 61, of which 31 were waited for; matrix products, arithmetic and copies ran while one was open for 16% of the time, Pallas kernels for 0%

profile of v1, /device:TPU:0, one launch (start us, length us, event | category | flops | bytes accessed | tf_op | source)
XLA Modules:
  0.0 373.4 jit_solution(14896819349369433020)
XLA Ops:
  2.4 3.0 collective-permute-start
  9.3 2.0 collective-permute-start.4
  11.3 10.7 %collective-permute-done = bf16[4,160,512]{2,1,0:T(8,128)(2,1)S(1)} collective-permute-done((bf16[4,160,512]{2,1,0:T(8,128)(2,1)}, bf16[4,160,512]{2,1,0:T(8,128)(2,1)S(1)}, u32[]{:S(2)}, u32[]{:S(2)}) %collective-permute-start) | collective-permute-done | bytes 655392 | tf_op jit(solution)/shard_map/ppermute | solution.py:39
  23.3 12.5 %collective-permute-done.2 = bf16[4,160,512]{2,1,0:T(8,128)(2,1)} collective-permute-done((bf16[4,160,512]{2,1,0:T(8,128)(2,1)}, bf16[4,160,512]{2,1,0:T(8,128)(2,1)}, u32[]{:S(2)}, u32[]{:S(2)}) %collective-permute-start.2) | collective-permute-done | bytes 655392 | tf_op jit(solution)/shard_map/ppermute | solution.py:39
  35.8 2.7 pad_maximum_fusion
  44.3 2.8 collective-permute-start.6
  51.1 28.2 %collective-permute-done.6 = bf16[704,512]{1,0:T(8,128)(2,1)} collective-permute-done((bf16[704,512]{1,0:T(8,128)(2,1)}, bf16[704,512]{1,0:T(8,128)(2,1)}, u32[]{:S(2)}, u32[]{:S(2)}) %collective-permute-start.6) | collective-permute-done | bytes 720928 | tf_op jit(solution)/shard_map/ppermute | solution.py:34
  82.4 5.4 %collective-permute-start.19 = (bf16[352,512]{1,0:T(8,128)(2,1)S(1)}, bf16[352,512]{1,0:T(8,128)(2,1)S(1)}, u32[]{:S(2)}, u32[]{:S(2)}) collective-permute-start(bf16[352,512]{1,0:T(8,128)(2,1)S(1)} %pad_maximum_fusion.11), channel_id=1, source_target_pairs={{0,8},{2,10},{4,12},{6,14},{8,0},{10,2},{12,4},{14,6},{1,9},{3,11}... | collective-permute-start | bytes 1081352 | tf_op jit(solution)/shard_map/ppermute | solution.py:34
  90.2 26.6 %collective-permute-done.19 = bf16[352,512]{1,0:T(8,128)(2,1)S(1)} collective-permute-done((bf16[352,512]{1,0:T(8,128)(2,1)S(1)}, bf16[352,512]{1,0:T(8,128)(2,1)S(1)}, u32[]{:S(2)}, u32[]{:S(2)}) %collective-permute-start.19) | collective-permute-done | bytes 360480 | tf_op jit(solution)/shard_map/ppermute | solution.py:34
  123.9 19.5 %collective-permute-done.5 = bf16[704,512]{1,0:T(8,128)(2,1)S(1)} collective-permute-done((bf16[704,512]{1,0:T(8,128)(2,1)}, bf16[704,512]{1,0:T(8,128)(2,1)S(1)}, u32[]{:S(2)}, u32[]{:S(2)}) %collective-permute-start.5) | collective-permute-done | bytes 720928 | tf_op jit(solution)/shard_map/ppermute | solution.py:34
  154.7 2.5 collective-permute-start.29
  158.6 2.5 collective-permute-start.23
  164.3 2.0 collective-permute-done.28
  171.4 2.0 collective-permute-done.22
  178.5 2.0 collective-permute-done.17
  184.0 2.7 collective-permute-done.12
  196.2 25.2 %collective-permute-done.30 = bf16[4,160,512]{2,1,0:T(8,128)(2,1)S(1)} collective-permute-done((bf16[4,160,512]{2,1,0:T(8,128)(2,1)S(1)}, bf16[4,160,512]{2,1,0:T(8,128)(2,1)S(1)}, u32[]{:S(2)}, u32[]{:S(2)}) %collective-permute-start.30) | collective-permute-done | bytes 655392 | tf_op jit(solution)/shard_map/ppermute | solution.py:39
  223.6 4.3 %collective-permute-done.34 = bf16[704,256]{1,0:T(8,128)(2,1)S(1)} collective-permute-done((bf16[704,256]{1,0:T(8,128)(2,1)S(1)}, bf16[704,256]{1,0:T(8,128)(2,1)S(1)}, u32[]{:S(2)}, u32[]{:S(2)}) %collective-permute-start.34) | collective-permute-done | bytes 360480 | tf_op jit(solution)/shard_map/ppermute | solution.py:27
  229.0 2.4 collective-permute-start.36
  234.6 29.6 %collective-permute-done.36 = bf16[704,512]{1,0:T(8,128)(2,1)} collective-permute-done((bf16[704,512]{1,0:T(8,128)(2,1)}, bf16[704,512]{1,0:T(8,128)(2,1)}, u32[]{:S(2)}, u32[]{:S(2)}) %collective-permute-start.36) | collective-permute-done | bytes 720928 | tf_op jit(solution)/shard_map/ppermute | solution.py:34
  267.0 3.7 collective-permute-start.49
  271.4 23.6 %collective-permute-done.49 = bf16[352,512]{1,0:T(8,128)(2,1)} collective-permute-done((bf16[352,512]{1,0:T(8,128)(2,1)}, bf16[352,512]{1,0:T(8,128)(2,1)}, u32[]{:S(2)}, u32[]{:S(2)}) %collective-permute-start.49) | collective-permute-done | bytes 360480 | tf_op jit(solution)/shard_map/ppermute | solution.py:34
  295.1 2.0 collective-permute-start.35
  302.5 3.4 constant_dynamic-update-slice_fusion.5
  305.9 2.2 fusion.19
  308.1 13.9 %collective-permute-done.35 = bf16[704,512]{1,0:T(8,128)(2,1)S(1)} collective-permute-done((bf16[704,512]{1,0:T(8,128)(2,1)}, bf16[704,512]{1,0:T(8,128)(2,1)S(1)}, u32[]{:S(2)}, u32[]{:S(2)}) %collective-permute-start.35) | collective-permute-done | bytes 720928 | tf_op jit(solution)/shard_map/ppermute | solution.py:34
  335.7 2.9 collective-permute-start.59
  339.5 2.9 collective-permute-start.53
  345.6 2.0 collective-permute-done.58
  352.7 2.0 collective-permute-done.52
  359.7 2.0 collective-permute-done.47
  364.9 3.0 collective-permute-done.42
  (253 shorter events, 120.0 us)
Async XLA Ops:
  2.4 19.6 %collective-permute-start = (bf16[4,160,512]{2,1,0:T(8,128)(2,1)}, bf16[4,160,512]{2,1,0:T(8,128)(2,1)S(1)}, u32[]{:S(2)}, u32[]{:S(2)}) collective-permute-start(bf16[4,160,512]{2,1,0:T(8,128)(2,1)} %bitcast.125), channel_id=1, source_target_pairs={{0,2},{2,0},{4,6},{6,4},{8,10},{10,8},{12,14},{14,12},{16,18},{18,... | collective-permute-start | bytes 1966088 | tf_op jit(solution)/shard_map/ppermute | solution.py:39
  5.4 17.9 %collective-permute-start.1 = (bf16[4,160,512]{2,1,0:T(8,128)(2,1)}, bf16[4,160,512]{2,1,0:T(8,128)(2,1)}, u32[]{:S(2)}, u32[]{:S(2)}) collective-permute-start(bf16[4,160,512]{2,1,0:T(8,128)(2,1)} %bitcast.125), channel_id=1, source_target_pairs={{0,16},{2,18},{4,20},{6,22},{8,24},{10,26},{12,28},{14,30},{16,0},... | collective-permute-start | bytes 1966088 | tf_op jit(solution)/shard_map/ppermute | solution.py:39
  6.9 28.9 %collective-permute-start.2 = (bf16[4,160,512]{2,1,0:T(8,128)(2,1)}, bf16[4,160,512]{2,1,0:T(8,128)(2,1)}, u32[]{:S(2)}, u32[]{:S(2)}) collective-permute-start(bf16[4,160,512]{2,1,0:T(8,128)(2,1)} %bitcast.125), channel_id=1, source_target_pairs={{0,18},{2,16},{4,22},{6,20},{8,26},{10,24},{12,30},{14,28},{16,2},... | collective-permute-start | bytes 1966088 | tf_op jit(solution)/shard_map/ppermute | solution.py:39
  9.3 32.9 %collective-permute-start.4 = (bf16[704,256]{1,0:T(8,128)(2,1)}, bf16[704,256]{1,0:T(8,128)(2,1)}, u32[]{:S(2)}, u32[]{:S(2)}) collective-permute-start(bf16[704,256]{1,0:T(8,128)(2,1)} %pad_maximum_fusion.10), channel_id=1, source_target_pairs={{0,2},{2,0},{4,6},{6,4},{8,10},{10,8},{12,14},{14,12},{1,3},{3,1},... | collective-permute-start | bytes 1081352 | tf_op jit(solution)/shard_map/ppermute | solution.py:27
  38.5 81.8 %collective-permute-start.3 = (bf16[4,640,512]{2,1,0:T(8,128)(2,1)}, bf16[4,640,512]{2,1,0:T(8,128)(2,1)}, u32[]{:S(2)}, u32[]{:S(2)}) collective-permute-start(bf16[4,640,512]{2,1,0:T(8,128)(2,1)} %pad_maximum_fusion), channel_id=1, source_target_pairs={{0,1},{1,0},{2,3},{3,2},{4,5},{5,4},{6,7},{7,6},{8,9},{9,8},{10,11... | collective-permute-start | bytes 7864328 | tf_op jit(solution)/shard_map/ppermute | solution.py:30
  44.3 35.1 %collective-permute-start.6 = (bf16[704,512]{1,0:T(8,128)(2,1)}, bf16[704,512]{1,0:T(8,128)(2,1)}, u32[]{:S(2)}, u32[]{:S(2)}) collective-permute-start(bf16[704,512]{1,0:T(8,128)(2,1)} %pad_maximum_fusion.3), channel_id=1, source_target_pairs={{0,8},{2,10},{4,12},{6,14},{8,0},{10,2},{12,4},{14,6},{1,9},{3,11}... | collective-permute-start | bytes 2162696 | tf_op jit(solution)/shard_map/ppermute | solution.py:34
  48.0 32.6 %collective-permute-start.9 = (bf16[352,256]{1,0:T(8,128)(2,1)S(1)}, bf16[352,256]{1,0:T(8,128)(2,1)}, u32[]{:S(2)}, u32[]{:S(2)}) collective-permute-start(bf16[352,256]{1,0:T(8,128)(2,1)S(1)} %constant_dynamic-slice_fusion.9), channel_id=1, source_target_pairs={{0,2},{2,0},{4,6},{6,4},{8,10},{10,8},{12,14},{14,12},{1,3},{3,1},... | collective-permute-start | bytes 540680 | tf_op jit(solution)/shard_map/ppermute | solution.py:27
  50.4 67.0 %collective-permute-start.7 = (bf16[704,512]{1,0:T(8,128)(2,1)}, bf16[704,512]{1,0:T(8,128)(2,1)S(1)}, u32[]{:S(2)}, u32[]{:S(2)}) collective-permute-start(bf16[704,512]{1,0:T(8,128)(2,1)} %pad_maximum_fusion.3), channel_id=1, source_target_pairs={{4,8},{6,10},{8,4},{10,6},{5,9},{7,11},{9,5},{11,7},{20,24},{22,26... | collective-permute-start | bytes 2162696 | tf_op jit(solution)/shard_map/ppermute | solution.py:34
  79.3 39.5 %collective-permute-start.8 = (bf16[704,512]{1,0:T(8,128)(2,1)}, bf16[704,512]{1,0:T(8,128)(2,1)S(1)}, u32[]{:S(2)}, u32[]{:S(2)}) collective-permute-start(bf16[704,512]{1,0:T(8,128)(2,1)} %collective-permute-done.6), channel_id=1, source_target_pairs={{4,0},{6,2},{8,12},{10,14},{5,1},{7,3},{9,13},{11,15},{20,16},{22,... | collective-permute-start | bytes 2162696 | tf_op jit(solution)/shard_map/ppermute | solution.py:80
  81.7 67.7 %collective-permute-start.24 = (bf16[352,512]{1,0:T(8,128)(2,1)S(1)}, bf16[352,512]{1,0:T(8,128)(2,1)S(1)}, u32[]{:S(2)}, u32[]{:S(2)}) collective-permute-start(bf16[352,512]{1,0:T(8,128)(2,1)S(1)} %pad_maximum_fusion.11), channel_id=1, source_target_pairs={{4,8},{6,10},{8,4},{10,6},{5,9},{7,11},{9,5},{11,7},{20,24},{22,26... | collective-permute-start | bytes 1081352 | tf_op jit(solution)/shard_map/ppermute | solution.py:34
  82.4 34.3 %collective-permute-start.19 = (bf16[352,512]{1,0:T(8,128)(2,1)S(1)}, bf16[352,512]{1,0:T(8,128)(2,1)S(1)}, u32[]{:S(2)}, u32[]{:S(2)}) collective-permute-start(bf16[352,512]{1,0:T(8,128)(2,1)S(1)} %pad_maximum_fusion.11), channel_id=1, source_target_pairs={{0,8},{2,10},{4,12},{6,14},{8,0},{10,2},{12,4},{14,6},{1,9},{3,11}... | collective-permute-start | bytes 1081352 | tf_op jit(solution)/shard_map/ppermute | solution.py:34
  116.8 35.2 %collective-permute-start.14 = (bf16[352,512]{1,0:T(8,128)(2,1)S(1)}, bf16[352,512]{1,0:T(8,128)(2,1)S(1)}, u32[]{:S(2)}, u32[]{:S(2)}) collective-permute-start(bf16[352,512]{1,0:T(8,128)(2,1)S(1)} %pad_maximum_fusion.11), channel_id=1, source_target_pairs={{0,4},{2,6},{4,0},{6,2},{8,12},{10,14},{12,8},{14,10},{1,5},{3,7},... | collective-permute-start | bytes 1081352 | tf_op jit(solution)/shard_map/ppermute | solution.py:34
  117.4 26.1 %collective-permute-start.5 = (bf16[704,512]{1,0:T(8,128)(2,1)}, bf16[704,512]{1,0:T(8,128)(2,1)S(1)}, u32[]{:S(2)}, u32[]{:S(2)}) collective-permute-start(bf16[704,512]{1,0:T(8,128)(2,1)} %pad_maximum_fusion.3), channel_id=1, source_target_pairs={{0,4},{2,6},{4,0},{6,2},{8,12},{10,14},{12,8},{14,10},{1,5},{3,7},... | collective-permute-start | bytes 2162696 | tf_op jit(solution)/shard_map/ppermute | solution.py:34
  118.8 30.6 %collective-permute-start.25 = (bf16[352,512]{1,0:T(8,128)(2,1)S(1)}, bf16[352,512]{1,0:T(8,128)(2,1)S(1)}, u32[]{:S(2)}, u32[]{:S(2)}) collective-permute-start(bf16[352,512]{1,0:T(8,128)(2,1)S(1)} %collective-permute-done.19), channel_id=1, source_target_pairs={{4,0},{6,2},{8,12},{10,14},{5,1},{7,3},{9,13},{11,15},{20,16},{22,... | collective-permute-start | bytes 1081352 | tf_op jit(solution)/shard_map/ppermute | solution.py:80
  162.8 12.5 %collective-permute-start.21 = (bf16[160,512]{1,0:T(8,128)(2,1)S(1)}, bf16[160,512]{1,0:T(8,128)(2,1)S(1)}, u32[]{:S(2)}, u32[]{:S(2)}) collective-permute-start(bf16[160,512]{1,0:T(8,128)(2,1)S(1)} %get-tuple-element.61), channel_id=1, source_target_pairs={{0,2},{2,0},{4,6},{6,4},{8,10},{10,8},{12,14},{14,12},{16,18},{18,... | collective-permute-start | bytes 491528 | tf_op jit(solution)/shard_map/ppermute | solution.py:39
  169.9 12.3 %collective-permute-start.16 = (bf16[160,512]{1,0:T(8,128)(2,1)S(1)}, bf16[160,512]{1,0:T(8,128)(2,1)S(1)}, u32[]{:S(2)}, u32[]{:S(2)}) collective-permute-start(bf16[160,512]{1,0:T(8,128)(2,1)S(1)} %get-tuple-element.58), channel_id=1, source_target_pairs={{0,2},{2,0},{4,6},{6,4},{8,10},{10,8},{12,14},{14,12},{16,18},{18,... | collective-permute-start | bytes 491528 | tf_op jit(solution)/shard_map/ppermute | solution.py:39
  189.8 31.7 %collective-permute-start.30 = (bf16[4,160,512]{2,1,0:T(8,128)(2,1)S(1)}, bf16[4,160,512]{2,1,0:T(8,128)(2,1)S(1)}, u32[]{:S(2)}, u32[]{:S(2)}) collective-permute-start(bf16[4,160,512]{2,1,0:T(8,128)(2,1)S(1)} %get-tuple-element.6), channel_id=1, source_target_pairs={{0,2},{2,0},{4,6},{6,4},{8,10},{10,8},{12,14},{14,12},{16,18},{18,... | collective-permute-start | bytes 1966088 | tf_op jit(solution)/shard_map/ppermute | solution.py:39
  191.1 30.4 %collective-permute-start.31 = (bf16[4,160,512]{2,1,0:T(8,128)(2,1)S(1)}, bf16[4,160,512]{2,1,0:T(8,128)(2,1)S(1)}, u32[]{:S(2)}, u32[]{:S(2)}) collective-permute-start(bf16[4,160,512]{2,1,0:T(8,128)(2,1)S(1)} %get-tuple-element.6), channel_id=1, source_target_pairs={{0,16},{2,18},{4,20},{6,22},{8,24},{10,26},{12,28},{14,30},{16,0},... | collective-permute-start | bytes 1966088 | tf_op jit(solution)/shard_map/ppermute | solution.py:39
  192.6 28.9 %collective-permute-start.32 = (bf16[4,160,512]{2,1,0:T(8,128)(2,1)S(1)}, bf16[4,160,512]{2,1,0:T(8,128)(2,1)S(1)}, u32[]{:S(2)}, u32[]{:S(2)}) collective-permute-start(bf16[4,160,512]{2,1,0:T(8,128)(2,1)S(1)} %get-tuple-element.6), channel_id=1, source_target_pairs={{0,18},{2,16},{4,22},{6,20},{8,26},{10,24},{12,30},{14,28},{16,2},... | collective-permute-start | bytes 1966088 | tf_op jit(solution)/shard_map/ppermute | solution.py:39
  194.4 33.5 %collective-permute-start.34 = (bf16[704,256]{1,0:T(8,128)(2,1)S(1)}, bf16[704,256]{1,0:T(8,128)(2,1)S(1)}, u32[]{:S(2)}, u32[]{:S(2)}) collective-permute-start(bf16[704,256]{1,0:T(8,128)(2,1)S(1)} %pad_maximum_fusion.13), channel_id=1, source_target_pairs={{0,2},{2,0},{4,6},{6,4},{8,10},{10,8},{12,14},{14,12},{1,3},{3,1},... | collective-permute-start | bytes 1081352 | tf_op jit(solution)/shard_map/ppermute | solution.py:27
  223.0 79.5 %collective-permute-start.33 = (bf16[4,640,512]{2,1,0:T(8,128)(2,1)}, bf16[4,640,512]{2,1,0:T(8,128)(2,1)}, u32[]{:S(2)}, u32[]{:S(2)}) collective-permute-start(bf16[4,640,512]{2,1,0:T(8,128)(2,1)} %pad_maximum_fusion.1), channel_id=1, source_target_pairs={{0,1},{1,0},{2,3},{3,2},{4,5},{5,4},{6,7},{7,6},{8,9},{9,8},{10,11... | collective-permute-start | bytes 7864328 | tf_op jit(solution)/shard_map/ppermute | solution.py:30
  229.0 35.2 %collective-permute-start.36 = (bf16[704,512]{1,0:T(8,128)(2,1)}, bf16[704,512]{1,0:T(8,128)(2,1)}, u32[]{:S(2)}, u32[]{:S(2)}) collective-permute-start(bf16[704,512]{1,0:T(8,128)(2,1)} %pad_maximum_fusion.4), channel_id=1, source_target_pairs={{0,8},{2,10},{4,12},{6,14},{8,0},{10,2},{12,4},{14,6},{1,9},{3,11}... | collective-permute-start | bytes 2162696 | tf_op jit(solution)/shard_map/ppermute | solution.py:34
  231.3 34.1 %collective-permute-start.39 = (bf16[352,256]{1,0:T(8,128)(2,1)S(1)}, bf16[352,256]{1,0:T(8,128)(2,1)S(1)}, u32[]{:S(2)}, u32[]{:S(2)}) collective-permute-start(bf16[352,256]{1,0:T(8,128)(2,1)S(1)} %constant_dynamic-slice_fusion.4), channel_id=1, source_target_pairs={{0,2},{2,0},{4,6},{6,4},{8,10},{10,8},{12,14},{14,12},{1,3},{3,1},... | collective-permute-start | bytes 540680 | tf_op jit(solution)/shard_map/ppermute | solution.py:27
  233.0 62.1 %collective-permute-start.37 = (bf16[704,512]{1,0:T(8,128)(2,1)}, bf16[704,512]{1,0:T(8,128)(2,1)}, u32[]{:S(2)}, u32[]{:S(2)}) collective-permute-start(bf16[704,512]{1,0:T(8,128)(2,1)} %pad_maximum_fusion.4), channel_id=1, source_target_pairs={{4,8},{6,10},{8,4},{10,6},{5,9},{7,11},{9,5},{11,7},{20,24},{22,26... | collective-permute-start | bytes 2162696 | tf_op jit(solution)/shard_map/ppermute | solution.py:34
  264.2 32.9 %collective-permute-start.38 = (bf16[704,512]{1,0:T(8,128)(2,1)}, bf16[704,512]{1,0:T(8,128)(2,1)}, u32[]{:S(2)}, u32[]{:S(2)}) collective-permute-start(bf16[704,512]{1,0:T(8,128)(2,1)} %collective-permute-done.36), channel_id=1, source_target_pairs={{4,0},{6,2},{8,12},{10,14},{5,1},{7,3},{9,13},{11,15},{20,16},{22,... | collective-permute-start | bytes 2162696 | tf_op jit(solution)/shard_map/ppermute | solution.py:80
  267.0 28.0 %collective-permute-start.49 = (bf16[352,512]{1,0:T(8,128)(2,1)}, bf16[352,512]{1,0:T(8,128)(2,1)}, u32[]{:S(2)}, u32[]{:S(2)}) collective-permute-start(bf16[352,512]{1,0:T(8,128)(2,1)} %pad_maximum_fusion.14), channel_id=1, source_target_pairs={{0,8},{2,10},{4,12},{6,14},{8,0},{10,2},{12,4},{14,6},{1,9},{3,11}... | collective-permute-start | bytes 1081352 | tf_op jit(solution)/shard_map/ppermute | solution.py:34
  270.7 58.6 %collective-permute-start.54 = (bf16[352,512]{1,0:T(8,128)(2,1)}, bf16[352,512]{1,0:T(8,128)(2,1)S(1)}, u32[]{:S(2)}, u32[]{:S(2)}) collective-permute-start(bf16[352,512]{1,0:T(8,128)(2,1)} %pad_maximum_fusion.14), channel_id=1, source_target_pairs={{4,8},{6,10},{8,4},{10,6},{5,9},{7,11},{9,5},{11,7},{20,24},{22,26... | collective-permute-start | bytes 1081352 | tf_op jit(solution)/shard_map/ppermute | solution.py:34
  295.1 37.8 %collective-permute-start.44 = (bf16[352,512]{1,0:T(8,128)(2,1)}, bf16[352,512]{1,0:T(8,128)(2,1)S(1)}, u32[]{:S(2)}, u32[]{:S(2)}) collective-permute-start(bf16[352,512]{1,0:T(8,128)(2,1)} %pad_maximum_fusion.14), channel_id=1, source_target_pairs={{0,4},{2,6},{4,0},{6,2},{8,12},{10,14},{12,8},{14,10},{1,5},{3,7},... | collective-permute-start | bytes 1081352 | tf_op jit(solution)/shard_map/ppermute | solution.py:34
  295.1 26.9 %collective-permute-start.35 = (bf16[704,512]{1,0:T(8,128)(2,1)}, bf16[704,512]{1,0:T(8,128)(2,1)S(1)}, u32[]{:S(2)}, u32[]{:S(2)}) collective-permute-start(bf16[704,512]{1,0:T(8,128)(2,1)} %pad_maximum_fusion.4), channel_id=1, source_target_pairs={{0,4},{2,6},{4,0},{6,2},{8,12},{10,14},{12,8},{14,10},{1,5},{3,7},... | collective-permute-start | bytes 2162696 | tf_op jit(solution)/shard_map/ppermute | solution.py:34
  297.1 32.2 %collective-permute-start.55 = (bf16[352,512]{1,0:T(8,128)(2,1)}, bf16[352,512]{1,0:T(8,128)(2,1)S(1)}, u32[]{:S(2)}, u32[]{:S(2)}) collective-permute-start(bf16[352,512]{1,0:T(8,128)(2,1)} %collective-permute-done.49), channel_id=1, source_target_pairs={{4,0},{6,2},{8,12},{10,14},{5,1},{7,3},{9,13},{11,15},{20,16},{22,... | collective-permute-start | bytes 1081352 | tf_op jit(solution)/shard_map/ppermute | solution.py:80
  343.7 12.9 %collective-permute-start.51 = (bf16[160,512]{1,0:T(8,128)(2,1)S(1)}, bf16[160,512]{1,0:T(8,128)(2,1)S(1)}, u32[]{:S(2)}, u32[]{:S(2)}) collective-permute-start(bf16[160,512]{1,0:T(8,128)(2,1)S(1)} %get-tuple-element.45), channel_id=1, source_target_pairs={{0,2},{2,0},{4,6},{6,4},{8,10},{10,8},{12,14},{14,12},{16,18},{18,... | collective-permute-start | bytes 491528 | tf_op jit(solution)/shard_map/ppermute | solution.py:39
  351.2 12.3 %collective-permute-start.46 = (bf16[160,512]{1,0:T(8,128)(2,1)S(1)}, bf16[160,512]{1,0:T(8,128)(2,1)S(1)}, u32[]{:S(2)}, u32[]{:S(2)}) collective-permute-start(bf16[160,512]{1,0:T(8,128)(2,1)S(1)} %get-tuple-element.42), channel_id=1, source_target_pairs={{0,2},{2,0},{4,6},{6,4},{8,10},{10,8},{12,14},{14,12},{16,18},{18,... | collective-permute-start | bytes 491528 | tf_op jit(solution)/shard_map/ppermute | solution.py:39
  (49 other events, 431.6 us)
